TPU v7x, 32 devices: a whole 2x2x4 slice. The times are simulated.
32 devices in a mesh: grp: 2 (over x), ep: 16 (over z, y, core).
Axes of the slice: x: 2, y: 2, z: 4, core: 2. Of those that a mesh axis runs over, the one named last changes fastest.
Arguments:
- tokens: bfloat16 [4096, 2048], P(('grp', 'ep')), parts along dimension 0, may hold values from -6 to 6
- routing: int32 [4096, 2], P(('grp', 'ep')), parts along dimension 0, may hold values from 0 to 3, all different within a row; in each aligned block of 128 rows (0 to 127, 128 to 255, ...) at most 80 rows name the same one
- gates: float32 [4096, 2], P(('grp', 'ep')), parts along dimension 0, may hold values from 0.2 to 1
- norm_gain: bfloat16 [2048], replicated, may hold values from 0.099609375 to 1.8984375
- w_gate: bfloat16 [16, 2048, 896], P('ep'), may hold values from -0.125 to 0.125
- w_up: bfloat16 [16, 2048, 896], P('ep'), may hold values from -0.125 to 0.125
- w_down: bfloat16 [16, 896, 2048], P('ep'), may hold values from -0.09375 to 0.09375
Outputs:
- mixed: bfloat16 [4096, 2048], P(('grp', 'ep')), parts along dimension 0
There are 2 independent parts, one for each index of `grp`. A program takes and returns all parts, laid end to end along the dimension named above; an argument that names none is the same for every part. Nothing has to cross between parts.
Inputs may be any that keep to these rules, and one draw needn't show every extreme that they name: `routing`: each row names 2 different experts. Among the rows of one device at most 80 name any one expert, and in every draw some expert is named by exactly 80 rows of some device.
All inputs are finite; a program needn't handle non-finite values.
Results may differ from a plain program's by a relative error of at most 0.0078.
Values may be sent and summed in bfloat16 or wider, within the bound.
A program may use at most 128 MiB of HBM per device.

v0:
```python
import functools

import jax
import jax.numpy as jnp
from jax import lax
from jax.experimental import pallas as pl
from jax.experimental.pallas import tpu as pltpu
from jax.sharding import PartitionSpec as P

GROUP = 4
LANE = 128
PIECES = 4


def kernel(n, cap, tok, rt, gt, gain, wg, wu, wd, out,
           normed, outgoing, xbuf, wgu, wdn, hidden, part, give, take, cross, crossed,
           finished, ret, total, table, w_sem, zs, zr, ys, yr, cs, cr, fs, fr, gs, gr, bs, br, es, er):
    toks, width = tok.shape
    ff = wg.shape[1]
    me = lax.axis_index("ep")
    g, j = me // GROUP, me % GROUP
    partner = g * GROUP + (j + 1 - 2 * (j % 2))
    across = g * GROUP + (j + 2) % GROUP
    sources = [(g + o) % n for o in range(n)]
    send_order = sorted(range(1, n), key=lambda o: min(o, n - o))
    span = width // PIECES

    def remote(src, dst, send, recv, device):
        return pltpu.make_async_remote_copy(
            src_ref=src, dst_ref=dst, send_sem=send, recv_sem=recv,
            device_id={"ep": device}, device_id_type=pl.DeviceIdType.MESH)

    barrier = pltpu.get_barrier_semaphore()
    others = [partner, across] + [s * GROUP + j for s in sources[1:]]
    for other in others:
        pl.semaphore_signal(barrier, inc=1, device_id={"ep": other},
                            device_id_type=pl.DeviceIdType.MESH)

    tiles = ff // LANE
    loads = []
    for t in range(tiles):
        loads.append(pltpu.make_async_copy(wg.at[:, pl.ds(t * LANE, LANE)], wgu.at[t, :, pl.ds(0, LANE)], w_sem.at[2 * t]))
        loads.append(pltpu.make_async_copy(wu.at[:, pl.ds(t * LANE, LANE)], wgu.at[t, :, pl.ds(LANE, LANE)], w_sem.at[2 * t + 1]))
    loads.append(pltpu.make_async_copy(wd, wdn, w_sem.at[2 * tiles]))
    for load in loads:
        load.start()

    values = tok[...].astype(jnp.float32)
    scale = lax.rsqrt(jnp.mean(values * values, axis=-1, keepdims=True) + 1e-06)
    normed[...] = (values * scale * gain[...].reshape(1, width).astype(jnp.float32)).astype(jnp.bfloat16)

    table[...] = jnp.zeros_like(table)
    table[0:2] = rt[...].astype(jnp.float32)
    table[2:4] = gt[...]
    turned = table[...].T
    first, second = turned[:, 0:1], turned[:, 1:2]
    experts_at = lax.broadcasted_iota(jnp.int32, (toks, LANE), 1).astype(jnp.float32)
    named = ((experts_at == first) | (experts_at == second)).astype(jnp.float32)
    lower = (lax.broadcasted_iota(jnp.int32, (toks, toks), 1)
             < lax.broadcasted_iota(jnp.int32, (toks, toks), 0)).astype(jnp.bfloat16)
    before = jnp.dot(lower, named.astype(jnp.bfloat16), preferred_element_type=jnp.float32)
    code = jnp.where(named > 0.5, before, -1.0)
    code_t = code.T

    def pack(e, dst):
        row = jnp.sum(jnp.where(lax.broadcasted_iota(jnp.int32, (LANE, toks), 0) == e, code_t, 0.0), axis=0, keepdims=True)
        slot = lax.broadcasted_iota(jnp.int32, (cap, toks), 0).astype(jnp.float32)
        pick = (slot == row).astype(jnp.bfloat16)

        def body(t, _):
            cols = pl.ds(pl.multiple_of(t * 512, 512), 512)
            dst[:, cols] = jnp.dot(pick, normed[:, cols], preferred_element_type=jnp.float32).astype(jnp.bfloat16)
            return _

        lax.fori_loop(0, width // 512, body, 0)

    def lane_rows(lane):
        return pl.ds(lane * cap, cap)

    waits = []

    def start(copy):
        copy.start()
        waits.append(copy)

    def across_copy(i):
        s = sources[i]
        return remote(xbuf.at[s, lane_rows(0)], xbuf.at[s, lane_rows(2)], ys.at[i], yr.at[i], across)

    def beside_copy(i):
        s = sources[i]
        return remote(xbuf.at[s, lane_rows(0)], xbuf.at[s, lane_rows(1)], cs.at[i], cr.at[i], partner)

    def forward_copy(i):
        s = sources[i]
        return remote(xbuf.at[s, lane_rows(2)], xbuf.at[s, lane_rows(3)], fs.at[i], fr.at[i], partner)

    def piece_of(h):
        return pl.ds(h * span, span)

    def give_copy(i, h):
        return remote(give.at[i, :, :, piece_of(h)], take.at[i, :, :, piece_of(h)],
                      gs.at[i, h], gr.at[i, h], partner)

    def cross_copy(i, h):
        return remote(cross.at[i, :, piece_of(h)], crossed.at[i, :, piece_of(h)],
                      bs.at[i, h], br.at[i, h], across)

    def arrive(i):
        if i:
            s = sources[i]
            remote(outgoing.at[0], xbuf.at[s, lane_rows(0)], zs.at[0], zr.at[s], partner).wait_recv()
        start(across_copy(i))
        start(beside_copy(i))

    def forward(i):
        across_copy(i).wait_recv()
        start(forward_copy(i))

    def rise(i):
        s = sources[i]
        beside_copy(i).wait_recv()
        forward_copy(i).wait_recv()

        def up(t, _):
            both = jnp.dot(xbuf[s], wgu[t], preferred_element_type=jnp.float32)
            gate_act, up_act = both[:, :LANE], both[:, LANE:]
            act = gate_act / (1.0 + jnp.exp(-gate_act)) * up_act
            hidden[:, pl.ds(pl.multiple_of(t * LANE, LANE), LANE)] = act.astype(jnp.bfloat16)
            return _

        lax.fori_loop(0, tiles, up, 0)

    def fall(i, h):
        slot = i % 2

        def down(t, _):
            cols = pl.ds(pl.multiple_of(h * span + t * 256, 256), 256)
            piece = jnp.dot(hidden[...], wdn[:, cols], preferred_element_type=jnp.float32)
            part[slot, 0, :, cols] = piece[0:cap]
            give[i, 0, :, cols] = piece[cap:2 * cap].astype(jnp.bfloat16)
            part[slot, 1, :, cols] = piece[2 * cap:3 * cap]
            give[i, 1, :, cols] = piece[3 * cap:4 * cap].astype(jnp.bfloat16)
            return _

        lax.fori_loop(0, span // 256, down, 0)
        start(give_copy(i, h))

    def reduce_pair(i, h):
        give_copy(i, h).wait_recv()
        cols = piece_of(h)
        cross[i, :, cols] = (part[i % 2, 1, :, cols] + take[i, 1, :, cols].astype(jnp.float32)).astype(jnp.bfloat16)
        start(cross_copy(i, h))

    def finish(i, h):
        cross_copy(i, h).wait_recv()
        cols = piece_of(h)
        done = (part[i % 2, 0, :, cols] + take[i, 0, :, cols].astype(jnp.float32)
                + crossed[i, :, cols].astype(jnp.float32)).astype(jnp.bfloat16)
        if i == 0:
            ret[g, :, cols] = done
        else:
            finished[i, :, cols] = done
            start(remote(finished.at[i, :, cols], ret.at[g, :, cols], es.at[i, h], er.at[g, h],
                         sources[i] * GROUP + j))

    def mix(i, h, last):
        e = sources[i]
        cols = piece_of(h)
        if i:
            remote(finished.at[i, :, cols], ret.at[e, :, cols], es.at[i, h], er.at[e, h], partner).wait_recv()
        column = jnp.sum(jnp.where(experts_at == e.astype(jnp.float32), code, 0.0), axis=1, keepdims=True)
        slot = lax.broadcasted_iota(jnp.int32, (toks, cap), 1).astype(jnp.float32)
        pick = (slot == column).astype(jnp.bfloat16)
        name = e.astype(jnp.float32)
        gate = jnp.where(first == name, turned[:, 2:3], 0.0) + jnp.where(second == name, turned[:, 3:4], 0.0)
        term = gate * jnp.dot(pick, ret[e, :, cols], preferred_element_type=jnp.float32)
        if i:
            term = total[:, cols] + term
        if last:
            out[:, cols] = term.astype(jnp.bfloat16)
        else:
            total[:, cols] = term

    pieces = range(PIECES)
    pack(g, xbuf.at[g, lane_rows(0)])
    pack(sources[send_order[0]], outgoing.at[send_order[0]])
    pl.semaphore_wait(barrier, len(others))
    arrive(0)
    for o in send_order:
        if o != send_order[0]:
            pack(sources[o], outgoing.at[o])
        start(remote(outgoing.at[o], xbuf.at[g, lane_rows(0)], zs.at[o], zr.at[g], sources[o] * GROUP + j))
    forward(0)
    arrive(1)
    for load in loads:
        load.wait()
    for i in range(n):
        rise(i)
        if i and i + 1 < n:
            arrive(i + 1)
        for h in pieces:
            fall(i, h)
            if h:
                reduce_pair(i, h - 1)
        reduce_pair(i, PIECES - 1)
        if i:
            for h in pieces:
                finish(i - 1, h)
        if i + 1 < n:
            forward(i + 1)
    order = [0] + [n - o for o in range(1, n)]
    for i in order[:-1]:
        if i == order[-2]:
            for h in pieces:
                finish(n - 1, h)
        for h in pieces:
            mix(i, h, False)
    for h in pieces:
        mix(order[-1], h, True)
    for copy in waits:
        copy.wait_send()


def per_device(tokens, routing, gates, norm_gain, w_gate, w_up, w_down):
    toks, width = tokens.shape
    top = routing.shape[1]
    devices = lax.axis_size("ep")
    n = devices // GROUP
    cap = GROUP * (5 * toks * top // (4 * devices))
    cap = -(-cap // 16) * 16
    ff = w_gate.shape[2]
    bf, f32 = jnp.bfloat16, jnp.float32
    dma = pltpu.SemaphoreType.DMA((n,))
    dmas = pltpu.SemaphoreType.DMA((n, PIECES))
    vmem = pl.BlockSpec(memory_space=pltpu.VMEM)
    hbm = pl.BlockSpec(memory_space=pl.ANY)
    return pl.pallas_call(
        functools.partial(kernel, n, cap),
        out_shape=jax.ShapeDtypeStruct((toks, width), bf),
        in_specs=[vmem] * 4 + [hbm] * 3,
        out_specs=vmem,
        scratch_shapes=[
            pltpu.VMEM((toks, width), bf),
            pltpu.VMEM((n, cap, width), bf),
            pltpu.VMEM((n, GROUP * cap, width), bf),
            pltpu.VMEM((ff // LANE, width, 2 * LANE), bf),
            pltpu.VMEM((ff, width), bf),
            pltpu.VMEM((GROUP * cap, ff), bf),
            pltpu.VMEM((2, 2, cap, width), f32),
            pltpu.VMEM((n, 2, cap, width), bf),
            pltpu.VMEM((n, 2, cap, width), bf),
            pltpu.VMEM((n, cap, width), bf),
            pltpu.VMEM((n, cap, width), bf),
            pltpu.VMEM((n, cap, width), bf),
            pltpu.VMEM((n, cap, width), bf),
            pltpu.VMEM((toks, width), f32),
            pltpu.VMEM((LANE, toks), f32),
            pltpu.SemaphoreType.DMA((2 * (ff // LANE) + 1,)),
        ] + [dma] * 8 + [dmas] * 6,
        compiler_params=pltpu.CompilerParams(
            collective_id=0, has_side_effects=True, vmem_limit_bytes=62 * 1024 * 1024),
    )(tokens, routing.T, gates.T, norm_gain, w_gate.reshape(w_gate.shape[1:]),
      w_up.reshape(w_up.shape[1:]), w_down.reshape(w_down.shape[1:]))


def solution(mesh):
    placed = (
        P(("grp", "ep"), None),
        P(("grp", "ep"), None),
        P(("grp", "ep"), None),
        P(),
        P("ep", None, None),
        P("ep", None, None),
        P("ep", None, None),
    )
    return jax.shard_map(
        per_device, mesh=mesh, in_specs=placed, out_specs=P(("grp", "ep"), None), check_vma=False
    )
```

profile of v0, /device:TPU:31, one launch (start us, length us, event | category | flops | bytes accessed | tf_op | source)
XLA Modules:
  0.0 95.3 jit_solution(11416333181633820590)
XLA Ops:
  0.0 93.4 %shard_map.73 = bf16[128,2048]{1,0:T(8,128)(2,1)} custom-call(bf16[128,2048]{1,0:T(8,128)(2,1)} %tok.1, s32[2,128]{1,0:T(2,128)} %bitcast.8, f32[2,128]{1,0:T(2,128)} %bitcast.9, bf16[2048]{0:T(1024)(128)(2,1)} %gain.1, bf16[2048,896]{1,0:T(8,128)(2,1)} %bitcast.5, bf16[2048,896]{1,0:T(8,128)(2,1)} %bitcast.6, bf16[896,2048]{1,0:T(8,128)(2,1)} %bitcast.7), custom_call_target="tpu_custom_call" | custom-call | tf_op jit(solution)/shard_map/pallas_call | solution.py:238
  93.4 1.9 %copy.9 = bf16[128,2048]{1,0:T(8,128)(2,1)} copy(bf16[128,2048]{1,0:T(8,128)(2,1)} %shard_map.73) | data formatting | bytes 1048576
where the time goes:
time: 95.4 us; the launch traced here: 95.3 us
  Pallas kernels  93.4 us (98%)
  local copies, waits for them, and re-layouts  1.88 us (2%)
    pallas_call x1, Pallas kernels, per_device(): pl.pallas_call(functools.partial(kernel, n, cap), out_shape=jax.ShapeDtyp...  93.4 us

commit v1 on v0

v1 whole, which is shorter than its diff:
```python
import functools

import jax
import jax.numpy as jnp
from jax import lax
from jax.experimental import pallas as pl
from jax.experimental.pallas import tpu as pltpu
from jax.sharding import PartitionSpec as P

GROUP = 4
LANE = 128
PIECES = 4
PARTS = 2


def kernel(n, cap, tok_in, rt_in, gt_in, gain_in, wg, wu, wd, out_to,
           tok, rt, gt, gain, out, normed, outgoing, xbuf, wgu, wdn, hidden, part, give, take, cross, crossed,
           finished, ret, total, table, turned, code, in_sem, w_sem, out_sem,
           zs, zr, ys, yr, cs, cr, fs, fr, gs, gr, bs, br, es, er):
    toks, width = tok.shape
    ff = wg.shape[1]
    me = lax.axis_index("ep")
    g, j = me // GROUP, me % GROUP
    partner = g * GROUP + (j + 1 - 2 * (j % 2))
    across = g * GROUP + (j + 2) % GROUP
    span = width // PIECES
    half = width // PARTS

    upper = (2 * g) // n
    edge = g + upper * (n - 1 - 2 * g)
    inner = 1 - 2 * upper

    def source(i):
        past = jnp.minimum(1, i // (2 * edge + 1))
        far = (1 - past) * ((i + 1) // 2) + past * (i - edge)
        way = past + (1 - past) * (2 * (i % 2) - 1)
        return g + inner * way * far

    def remote(src, dst, send, recv, device):
        return pltpu.make_async_remote_copy(
            src_ref=src, dst_ref=dst, send_sem=send, recv_sem=recv,
            device_id={"ep": device}, device_id_type=pl.DeviceIdType.MESH)

    barrier = pltpu.get_barrier_semaphore()
    others = [partner, across] + [source(i) * GROUP + j for i in range(1, n)]
    for other in others:
        pl.semaphore_signal(barrier, inc=1, device_id={"ep": other},
                            device_id_type=pl.DeviceIdType.MESH)

    inputs = [pltpu.make_async_copy(a, b, in_sem.at[k])
              for k, (a, b) in enumerate([(tok_in, tok), (rt_in, rt), (gt_in, gt), (gain_in, gain)])]
    for copy in inputs:
        copy.start()
    tiles = ff // LANE
    loads = []
    for t in range(tiles):
        loads.append(pltpu.make_async_copy(wg.at[:, pl.ds(t * LANE, LANE)], wgu.at[t, :, pl.ds(0, LANE)], w_sem.at[2 * t]))
        loads.append(pltpu.make_async_copy(wu.at[:, pl.ds(t * LANE, LANE)], wgu.at[t, :, pl.ds(LANE, LANE)], w_sem.at[2 * t + 1]))
    loads.append(pltpu.make_async_copy(wd, wdn, w_sem.at[2 * tiles]))
    table[...] = jnp.zeros_like(table)
    for copy in inputs:
        copy.wait()
    for copy in loads:
        copy.start()

    values = tok[...].astype(jnp.float32)
    scale = lax.rsqrt(jnp.mean(values * values, axis=-1, keepdims=True) + 1e-06)
    normed[...] = (values * scale * gain[...].reshape(1, width).astype(jnp.float32)).astype(jnp.bfloat16)

    table[0:2] = rt[...].astype(jnp.float32)
    table[2:4] = gt[...]
    turned[...] = table[...].T
    experts_at = lax.broadcasted_iota(jnp.int32, (toks, LANE), 1).astype(jnp.float32)
    named = ((experts_at == turned[:, 0:1]) | (experts_at == turned[:, 1:2])).astype(jnp.float32)
    lower = (lax.broadcasted_iota(jnp.int32, (toks, toks), 1)
             < lax.broadcasted_iota(jnp.int32, (toks, toks), 0)).astype(jnp.bfloat16)
    before = jnp.dot(lower, named.astype(jnp.bfloat16), preferred_element_type=jnp.float32)
    code[...] = jnp.where(named > 0.5, before, -1.0)
    table[...] = code[...].T

    def pack(e, dst):
        row = jnp.sum(jnp.where(lax.broadcasted_iota(jnp.int32, (LANE, toks), 0) == e, table[...], 0.0), axis=0, keepdims=True)
        slot = lax.broadcasted_iota(jnp.int32, (cap, toks), 0).astype(jnp.float32)
        pick = (slot == row).astype(jnp.bfloat16)
        for t in range(width // 512):
            cols = pl.ds(t * 512, 512)
            dst[:, cols] = jnp.dot(pick, normed[:, cols], preferred_element_type=jnp.float32).astype(jnp.bfloat16)

    def lane_rows(lane, count=1):
        return pl.ds(pl.multiple_of(lane * cap, cap), count * cap)

    def part_of(p):
        return pl.ds(p * half, half)

    def piece_of(h):
        return pl.ds(h * span, span)

    def lane_copy(i, p, src, dst, send, recv, device):
        s = source(i)
        return remote(xbuf.at[s, lane_rows(src), part_of(p)], xbuf.at[s, lane_rows(dst), part_of(p)],
                      send.at[i, p], recv.at[i, p], device)

    def across_copy(i, p):
        return lane_copy(i, p, 0, 2, ys, yr, across)

    def beside_copy(i, p):
        return lane_copy(i, p, 0, 1, cs, cr, partner)

    def forward_copy(i, p):
        return lane_copy(i, p, 2, 3, fs, fr, partner)

    def source_copy(i, p, to, at):
        return remote(outgoing.at[i, :, part_of(p)], xbuf.at[at, lane_rows(0), part_of(p)],
                      zs.at[i, p], zr.at[at, p], to * GROUP + j)

    def give_copy(i, side, h):
        return remote(give.at[i, side, :, piece_of(h)], take.at[i, side, :, piece_of(h)],
                      gs.at[2 * i + side, h], gr.at[2 * i + side, h], partner)

    def cross_copy(i, h):
        return remote(cross.at[i, :, piece_of(h)], crossed.at[i, :, piece_of(h)],
                      bs.at[i, h], br.at[i, h], across)

    def return_copy(i, h, to, at):
        return remote(finished.at[i, :, piece_of(h)], ret.at[at, :, piece_of(h)],
                      es.at[i, h], er.at[at, h], to * GROUP + j)

    def depart(i):
        for p in range(PARTS):
            source_copy(i, p, source(i), g).start()

    def relay(i, p):
        source_copy(i, p, partner // GROUP, source(i)).wait_recv()
        across_copy(i, p).start()
        beside_copy(i, p).start()

    def forward(i, p):
        across_copy(i, p).wait_recv()
        forward_copy(i, p).start()

    def rise(i, side):
        rows = xbuf[source(i), lane_rows(2 * side, 2)]
        for t in range(tiles):
            both = jnp.dot(rows, wgu[t], preferred_element_type=jnp.float32)
            gate_act, up_act = both[:, :LANE], both[:, LANE:]
            act = gate_act / (1.0 + jnp.exp(-gate_act)) * up_act
            hidden[:, pl.ds(t * LANE, LANE)] = act.astype(jnp.bfloat16)

    def fall(i, side):
        for h in pieces:
            cols = piece_of(h)
            piece = jnp.dot(hidden[...], wdn[:, cols], preferred_element_type=jnp.float32)
            part[i, side, :, cols] = piece[0:cap]
            give[i, side, :, cols] = piece[cap:2 * cap].astype(jnp.bfloat16)
        for h in pieces:
            give_copy(i, side, h).start()

    def reduce_pair(i, h, send):
        give_copy(i, 1, h).wait_recv()
        cols = piece_of(h)
        cross[i, :, cols] = (part[i, 1, :, cols] + take[i, 1, :, cols].astype(jnp.float32)).astype(jnp.bfloat16)
        if send:
            cross_copy(i, h).start()

    def send_cross(i):
        for h in pieces:
            cross_copy(i, h).start()

    def finish(i, h):
        give_copy(i, 0, h).wait_recv()
        cross_copy(i, h).wait_recv()
        cols = piece_of(h)
        done = (part[i, 0, :, cols] + take[i, 0, :, cols].astype(jnp.float32)
                + crossed[i, :, cols].astype(jnp.float32)).astype(jnp.bfloat16)
        if i == 0:
            ret[g, :, cols] = done
        else:
            finished[i, :, cols] = done
            return_copy(i, h, source(i), g).start()

    def mixer(i):
        e = source(i)
        experts_at = lax.broadcasted_iota(jnp.int32, (toks, LANE), 1)
        column = jnp.sum(jnp.where(experts_at == e, code[...], 0.0), axis=1, keepdims=True)
        slot = lax.broadcasted_iota(jnp.int32, (toks, cap), 1).astype(jnp.float32)
        pick = (slot == column).astype(jnp.bfloat16)
        name = e.astype(jnp.float32)
        gate = (jnp.where(turned[:, 0:1] == name, turned[:, 2:3], 0.0)
                + jnp.where(turned[:, 1:2] == name, turned[:, 3:4], 0.0))
        def mix(h, start, last):
            cols = piece_of(h)
            if i:
                return_copy(i, h, partner // GROUP, e).wait_recv()
            term = gate * jnp.dot(pick, ret[e, :, cols], preferred_element_type=jnp.float32)
            if not start:
                term = total[:, cols] + term
            if last:
                out[:, cols] = term.astype(jnp.bfloat16)
                pltpu.make_async_copy(out.at[:, cols], out_to.at[:, cols], out_sem.at[h]).start()
            else:
                total[:, cols] = term

        return mix

    def mix_all(i, start, last):
        mix = mixer(i)
        for h in pieces:
            mix(h, start, last)

    def own(last):
        mix = mixer(0)
        for h in pieces:
            finish(0, h)
            mix(h, False, last)

    pieces = range(PIECES)
    parts = range(PARTS)
    at_edge, within = edge == 0, edge > 0
    pack(g, xbuf.at[g, lane_rows(0)])
    pack(source(1), outgoing.at[1])
    pl.semaphore_wait(barrier, len(others))
    for p in parts:
        across_copy(0, p).start()
        beside_copy(0, p).start()
    depart(1)
    for i in range(2, n):
        pack(source(i), outgoing.at[i])

        @pl.when(within)
        def _():
            depart(i)
    for load in loads:
        load.wait()

    def step(k, carry):
        def at(c):
            return pl.when(k == c)

        def when_is(c):
            return (k == c).astype(jnp.int32)

        i = k // 2 + when_is(1) - when_is(3)
        side = k % 2 + when_is(2) - when_is(1)

        @at(1)
        def _():
            for p in parts:
                forward(0, p)
                relay(1, p)

            @pl.when(within)
            def _():
                for p in parts:
                    relay(2, p)

        @at(2)
        def _():
            for p in parts:
                forward(1, p)

                @pl.when(at_edge)
                def _():
                    relay(2, p)

            @pl.when(at_edge)
            def _():
                for o in range(2, n):
                    depart(o)

        for o in range(3, n):
            @at(2 * o - 2)
            def _():
                @pl.when(within)
                def _():
                    relay(o, 0)

            @at(2 * o - 1)
            def _():
                for p in parts:
                    forward(o - 1, p)

                @pl.when(within)
                def _():
                    for p in parts[1:]:
                        relay(o, p)
                    if o == 3:
                        send_cross(1)

            @at(2 * o)
            def _():
                @pl.when(at_edge)
                def _():
                    for h in pieces[:-1]:
                        finish(o - 2, h)
                    relay(o, 0)
                    finish(o - 2, PIECES - 1)
                    for p in parts[1:]:
                        relay(o, p)
                if o < n - 1:
                    @pl.when(within)
                    def _():
                        for h in pieces:
                            finish(o - 2, h)

        @at(2 * n - 1)
        def _():
            for p in parts:
                forward(n - 1, p)

            @pl.when(within)
            def _():
                for h in pieces[:PIECES // 2]:
                    finish(n - 3, h)

        @pl.when(side == 0)
        def _():
            for p in parts:
                beside_copy(i, p).wait_recv()

        @pl.when(side == 1)
        def _():
            for p in parts:
                forward_copy(i, p).wait_recv()
        rise(i, side)

        @at(3)
        def _():
            for h in pieces:
                reduce_pair(1, h, False)

            @pl.when(at_edge)
            def _():
                send_cross(1)

        @at(4)
        def _():
            for h in pieces:
                reduce_pair(0, h, False)
        for o in range(3, n):
            @at(2 * o)
            def _():
                for h in pieces:
                    reduce_pair(o - 1, h, True)

        @at(2 * n - 1)
        def _():
            @pl.when(within)
            def _():
                for h in pieces[PIECES // 2:]:
                    finish(n - 3, h)
        fall(i, side)
        return carry

    lax.fori_loop(0, 2 * n, step, 0)
    for h in pieces[:PIECES // 2]:
        finish(n - 2, h)
    for h in pieces:
        reduce_pair(n - 1, h, True)
    send_cross(0)
    for h in pieces[PIECES // 2:]:
        finish(n - 2, h)
    for h in pieces:
        finish(n - 1, h)
    mix_all(1, True, False)

    @pl.when(at_edge)
    def _():
        own(False)
        for i in range(n - 1, 1, -1):
            mix_all(i, False, i == 2)

    @pl.when(within)
    def _():
        for i in range(2, n):
            mix_all(i, False, False)
        own(True)
    for h in pieces:
        pltpu.make_async_copy(out.at[:, piece_of(h)], out_to.at[:, piece_of(h)], out_sem.at[h]).wait()
    for i in range(n):
        for p in parts:
            across_copy(i, p).wait_send()
            beside_copy(i, p).wait_send()
            forward_copy(i, p).wait_send()
            if i:
                source_copy(i, p, source(i), g).wait_send()
        for h in pieces:
            give_copy(i, 0, h).wait_send()
            give_copy(i, 1, h).wait_send()
            cross_copy(i, h).wait_send()
            if i:
                return_copy(i, h, source(i), g).wait_send()


def per_device(tokens, routing, gates, norm_gain, w_gate, w_up, w_down):
    toks, width = tokens.shape
    top = routing.shape[1]
    devices = lax.axis_size("ep")
    n = devices // GROUP
    cap = GROUP * (5 * toks * top // (4 * devices))
    cap = -(-cap // 16) * 16
    ff = w_gate.shape[2]
    bf, f32 = jnp.bfloat16, jnp.float32
    by_part = pltpu.SemaphoreType.DMA((n, PARTS))
    by_side = pltpu.SemaphoreType.DMA((2 * n, PIECES))
    by_piece = pltpu.SemaphoreType.DMA((n, PIECES))
    hbm = pl.BlockSpec(memory_space=pl.ANY)
    return pl.pallas_call(
        functools.partial(kernel, n, cap),
        out_shape=jax.ShapeDtypeStruct((toks, width), bf),
        in_specs=[hbm] * 7,
        out_specs=hbm,
        scratch_shapes=[
            pltpu.VMEM((toks, width), bf),
            pltpu.VMEM((top, toks), jnp.int32),
            pltpu.VMEM((top, toks), f32),
            pltpu.VMEM((width,), bf),
            pltpu.VMEM((toks, width), bf),
            pltpu.VMEM((toks, width), bf),
            pltpu.VMEM((n, cap, width), bf),
            pltpu.VMEM((n, GROUP * cap, width), bf),
            pltpu.VMEM((ff // LANE, width, 2 * LANE), bf),
            pltpu.VMEM((ff, width), bf),
            pltpu.VMEM((2 * cap, ff), bf),
            pltpu.VMEM((n, 2, cap, width), f32),
            pltpu.VMEM((n, 2, cap, width), bf),
            pltpu.VMEM((n, 2, cap, width), bf),
            pltpu.VMEM((n, cap, width), bf),
            pltpu.VMEM((n, cap, width), bf),
            pltpu.VMEM((n, cap, width), bf),
            pltpu.VMEM((n, cap, width), bf),
            pltpu.VMEM((toks, width), f32),
            pltpu.VMEM((LANE, toks), f32),
            pltpu.VMEM((toks, LANE), f32),
            pltpu.VMEM((toks, LANE), f32),
            pltpu.SemaphoreType.DMA((4,)),
            pltpu.SemaphoreType.DMA((2 * (ff // LANE) + 1,)),
            pltpu.SemaphoreType.DMA((PIECES,)),
        ] + [by_part] * 8 + [by_side] * 2 + [by_piece] * 4,
        compiler_params=pltpu.CompilerParams(
            collective_id=0, has_side_effects=True, vmem_limit_bytes=62 * 1024 * 1024),
    )(tokens, routing.T, gates.T, norm_gain, w_gate.reshape(w_gate.shape[1:]),
      w_up.reshape(w_up.shape[1:]), w_down.reshape(w_down.shape[1:]))


def solution(mesh):
    placed = (
        P(("grp", "ep"), None),
        P(("grp", "ep"), None),
        P(("grp", "ep"), None),
        P(),
        P("ep", None, None),
        P("ep", None, None),
        P("ep", None, None),
    )
    return jax.shard_map(
        per_device, mesh=mesh, in_specs=placed, out_specs=P(("grp", "ep"), None), check_vma=False
    )
```

time: 95.4 us -> 76.5 us (0.80)
  the two profiles are of different devices: /device:TPU:31 before, /device:TPU:0 now
where the time goes in v1:
time: 76.5 us; the launch traced here: 76.3 us
  Pallas kernels  74.4 us (97%)
  local copies, waits for them, and re-layouts  1.88 us (2%)
    pallas_call x1, Pallas kernels, per_device(): pl.pallas_call(functools.partial(kernel, n, cap), out_shape=jax.ShapeDtyp...  74.4 us
    unnamed x1, local copies, waits for them, and re-layouts  1.88 us

profile of v1, /device:TPU:0, one launch (start us, length us, event | category | flops | bytes accessed | tf_op | source)
XLA Modules:
  0.0 76.3 jit_solution(4579553480611038577)
XLA Ops:
  0.0 74.4 %shard_map.73 = bf16[128,2048]{1,0:T(8,128)(2,1)} custom-call(bf16[128,2048]{1,0:T(8,128)(2,1)} %tok_in.1, s32[2,128]{1,0:T(2,128)} %bitcast.8, f32[2,128]{1,0:T(2,128)} %bitcast.9, bf16[2048]{0:T(1024)(128)(2,1)} %gain_in.1, bf16[2048,896]{1,0:T(8,128)(2,1)} %bitcast.5, bf16[2048,896]{1,0:T(8,128)(2,1)} %bitcast.6, bf16[896,2048]{1,0:T(8,128)(2,1)} %bitcast.7), custom_call_target="tpu_custom_call" | custom-call | tf_op jit(solution)/shard_map/pallas_call | solution.py:407
  74.4 1.9 %copy.9 = bf16[128,2048]{1,0:T(8,128)(2,1)} copy(bf16[128,2048]{1,0:T(8,128)(2,1)} %shard_map.73) | data formatting | bytes 1048576

commit v2 on v1

--- a/solution.py
+++ b/solution.py
@@ -48,7 +48,7 @@
                             device_id_type=pl.DeviceIdType.MESH)
 
     inputs = [pltpu.make_async_copy(a, b, in_sem.at[k])
-              for k, (a, b) in enumerate([(tok_in, tok), (rt_in, rt), (gt_in, gt), (gain_in, gain)])]
+              for k, (a, b) in enumerate([(tok_in, tok), (gain_in, gain), (rt_in, rt), (gt_in, gt)])]
     for copy in inputs:
         copy.start()
     tiles = ff // LANE
@@ -58,15 +58,8 @@
         loads.append(pltpu.make_async_copy(wu.at[:, pl.ds(t * LANE, LANE)], wgu.at[t, :, pl.ds(LANE, LANE)], w_sem.at[2 * t + 1]))
     loads.append(pltpu.make_async_copy(wd, wdn, w_sem.at[2 * tiles]))
     table[...] = jnp.zeros_like(table)
-    for copy in inputs:
+    for copy in inputs[2:]:
         copy.wait()
-    for copy in loads:
-        copy.start()
-
-    values = tok[...].astype(jnp.float32)
-    scale = lax.rsqrt(jnp.mean(values * values, axis=-1, keepdims=True) + 1e-06)
-    normed[...] = (values * scale * gain[...].reshape(1, width).astype(jnp.float32)).astype(jnp.bfloat16)
-
     table[0:2] = rt[...].astype(jnp.float32)
     table[2:4] = gt[...]
     turned[...] = table[...].T
@@ -77,6 +70,14 @@
     before = jnp.dot(lower, named.astype(jnp.bfloat16), preferred_element_type=jnp.float32)
     code[...] = jnp.where(named > 0.5, before, -1.0)
     table[...] = code[...].T
+
+    for copy in inputs[:2]:
+        copy.wait()
+    for copy in loads:
+        copy.start()
+    values = tok[...].astype(jnp.float32)
+    scale = lax.rsqrt(jnp.mean(values * values, axis=-1, keepdims=True) + 1e-06)
+    normed[...] = (values * scale * gain[...].reshape(1, width).astype(jnp.float32)).astype(jnp.bfloat16)
 
     def pack(e, dst):
         row = jnp.sum(jnp.where(lax.broadcasted_iota(jnp.int32, (LANE, toks), 0) == e, table[...], 0.0), axis=0, keepdims=True)
@@ -177,6 +178,9 @@
         else:
             finished[i, :, cols] = done
             return_copy(i, h, source(i), g).start()
+
+    def returned(i, h):
+        return_copy(i, h, partner // GROUP, source(i)).wait_recv()
 
     def mixer(i):
         e = source(i)
@@ -190,7 +194,7 @@
         def mix(h, start, last):
             cols = piece_of(h)
             if i:
-                return_copy(i, h, partner // GROUP, e).wait_recv()
+                returned(i, h)
             term = gate * jnp.dot(pick, ret[e, :, cols], preferred_element_type=jnp.float32)
             if not start:
                 term = total[:, cols] + term
@@ -207,11 +211,11 @@
         for h in pieces:
             mix(h, start, last)
 
-    def own(last):
+    def own(start, last):
         mix = mixer(0)
         for h in pieces:
             finish(0, h)
-            mix(h, False, last)
+            mix(h, start, last)
 
     pieces = range(PIECES)
     parts = range(PARTS)
@@ -239,8 +243,8 @@
         def when_is(c):
             return (k == c).astype(jnp.int32)
 
-        i = k // 2 + when_is(1) - when_is(3)
-        side = k % 2 + when_is(2) - when_is(1)
+        i = k // 2 + when_is(1) + when_is(3) - 2 * when_is(5)
+        side = k % 2 + when_is(2) + when_is(4) - when_is(1) - when_is(3)
 
         @at(1)
         def _():
@@ -261,56 +265,51 @@
                 @pl.when(at_edge)
                 def _():
                     relay(2, p)
-
-            @pl.when(at_edge)
-            def _():
-                for o in range(2, n):
-                    depart(o)
+                    if p == 0:
+                        for o in range(2, n):
+                            depart(o)
+
+        @at(4)
+        def _():
+            for p in parts:
+                forward(2, p)
 
         for o in range(3, n):
-            @at(2 * o - 2)
-            def _():
+            @at(2 * o - 1)
+            def _():
+                if o > 3:
+                    for p in parts:
+                        forward(o - 1, p)
+
                 @pl.when(within)
                 def _():
+                    for p in parts:
+                        relay(o, p)
+
+            @at(2 * o)
+            def _():
+                for h in pieces[:-1]:
+                    finish(o - 2, h)
+
+                @pl.when(at_edge)
+                def _():
                     relay(o, 0)
-
-            @at(2 * o - 1)
-            def _():
-                for p in parts:
-                    forward(o - 1, p)
-
-                @pl.when(within)
+                finish(o - 2, PIECES - 1)
+
+                @pl.when(at_edge)
                 def _():
                     for p in parts[1:]:
                         relay(o, p)
-                    if o == 3:
-                        send_cross(1)
-
-            @at(2 * o)
-            def _():
-                @pl.when(at_edge)
-                def _():
-                    for h in pieces[:-1]:
-                        finish(o - 2, h)
-                    relay(o, 0)
-                    finish(o - 2, PIECES - 1)
-                    for p in parts[1:]:
-                        relay(o, p)
-                if o < n - 1:
-                    @pl.when(within)
-                    def _():
-                        for h in pieces:
-                            finish(o - 2, h)
 
         @at(2 * n - 1)
         def _():
+            @pl.when(at_edge)
+            def _():
+                send_cross(0)
+                for h in pieces:
+                    finish(n - 2, h)
             for p in parts:
                 forward(n - 1, p)
-
-            @pl.when(within)
-            def _():
-                for h in pieces[:PIECES // 2]:
-                    finish(n - 3, h)
 
         @pl.when(side == 0)
         def _():
@@ -323,57 +322,45 @@
                 forward_copy(i, p).wait_recv()
         rise(i, side)
 
-        @at(3)
-        def _():
-            for h in pieces:
-                reduce_pair(1, h, False)
-
-            @pl.when(at_edge)
-            def _():
-                send_cross(1)
-
-        @at(4)
-        def _():
-            for h in pieces:
-                reduce_pair(0, h, False)
-        for o in range(3, n):
-            @at(2 * o)
+        @at(2 * n - 1)
+        def _():
+            @pl.when(within)
+            def _():
+                finish(n - 2, 0)
+        for o in range(n - 1):
+            @at(6 if o == 0 else 3 if o == 1 else 5 if o == 2 else 2 * o + 2)
             def _():
                 for h in pieces:
-                    reduce_pair(o - 1, h, True)
-
-        @at(2 * n - 1)
-        def _():
-            @pl.when(within)
-            def _():
-                for h in pieces[PIECES // 2:]:
-                    finish(n - 3, h)
+                    reduce_pair(o, h, o > 0)
         fall(i, side)
         return carry
 
     lax.fori_loop(0, 2 * n, step, 0)
-    for h in pieces[:PIECES // 2]:
-        finish(n - 2, h)
-    for h in pieces:
-        reduce_pair(n - 1, h, True)
-    send_cross(0)
-    for h in pieces[PIECES // 2:]:
-        finish(n - 2, h)
-    for h in pieces:
-        finish(n - 1, h)
-    mix_all(1, True, False)
-
     @pl.when(at_edge)
     def _():
-        own(False)
-        for i in range(n - 1, 1, -1):
-            mix_all(i, False, i == 2)
+        for h in pieces:
+            reduce_pair(n - 1, h, True)
+        own(True, False)
+        for h in pieces:
+            finish(n - 1, h)
+        mixers = [mixer(i) for i in range(1, n)]
+        for h in pieces:
+            for mix in mixers:
+                mix(h, False, mix is mixers[-1])
 
     @pl.when(within)
     def _():
-        for i in range(2, n):
-            mix_all(i, False, False)
-        own(True)
+        finish(n - 2, 1)
+        for h in pieces:
+            reduce_pair(n - 1, h, True)
+        send_cross(0)
+        for h in pieces[2:]:
+            finish(n - 2, h)
+        for h in pieces:
+            finish(n - 1, h)
+        for i in range(1, n):
+            mix_all(i, i == 1, False)
+        own(False, True)
     for h in pieces:
         pltpu.make_async_copy(out.at[:, piece_of(h)], out_to.at[:, piece_of(h)], out_sem.at[h]).wait()
     for i in range(n):

time: 76.5 us -> 73.6 us (0.962)
  Pallas kernels: 74.4 us -> 71.5 us
    pallas_call x1, Pallas kernels: 74.4 us -> 71.5 us  [per_device(): pl.pallas_call(functools.partial(kernel, n, cap), out_shape=jax.ShapeDtyp...]
where the time goes in v2:
time: 73.6 us; the launch traced here: 73.4 us
  Pallas kernels  71.5 us (97%)
  local copies, waits for them, and re-layouts  1.88 us (3%)
    pallas_call x1, Pallas kernels, per_device(): pl.pallas_call(functools.partial(kernel, n, cap), out_shape=jax.ShapeDtyp...  71.5 us
    unnamed x1, local copies, waits for them, and re-layouts  1.88 us

profile of v2, /device:TPU:0, one launch (start us, length us, event | category | flops | bytes accessed | tf_op | source)
XLA Modules:
  0.0 73.4 jit_solution(1632082517998649416)
XLA Ops:
  0.0 71.5 %shard_map.73 = bf16[128,2048]{1,0:T(8,128)(2,1)} custom-call(bf16[128,2048]{1,0:T(8,128)(2,1)} %tok_in.1, s32[2,128]{1,0:T(2,128)} %bitcast.8, f32[2,128]{1,0:T(2,128)} %bitcast.9, bf16[2048]{0:T(1024)(128)(2,1)} %gain_in.1, bf16[2048,896]{1,0:T(8,128)(2,1)} %bitcast.5, bf16[2048,896]{1,0:T(8,128)(2,1)} %bitcast.6, bf16[896,2048]{1,0:T(8,128)(2,1)} %bitcast.7), custom_call_target="tpu_custom_call" | custom-call | tf_op jit(solution)/shard_map/pallas_call | solution.py:394
  71.5 1.9 %copy.9 = bf16[128,2048]{1,0:T(8,128)(2,1)} copy(bf16[128,2048]{1,0:T(8,128)(2,1)} %shard_map.73) | data formatting | bytes 1048576

commit v3 on v2

--- a/solution.py
+++ b/solution.py
@@ -16,7 +16,7 @@
 def kernel(n, cap, tok_in, rt_in, gt_in, gain_in, wg, wu, wd, out_to,
            tok, rt, gt, gain, out, normed, outgoing, xbuf, wgu, wdn, hidden, part, give, take, cross, crossed,
            finished, ret, total, table, turned, code, in_sem, w_sem, out_sem,
-           zs, zr, ys, yr, cs, cr, fs, fr, gs, gr, bs, br, es, er):
+           sent, zr, yr, cr, fr, lr, gr, br, er):
     toks, width = tok.shape
     ff = wg.shape[1]
     me = lax.axis_index("ep")
@@ -54,9 +54,9 @@
     tiles = ff // LANE
     loads = []
     for t in range(tiles):
-        loads.append(pltpu.make_async_copy(wg.at[:, pl.ds(t * LANE, LANE)], wgu.at[t, :, pl.ds(0, LANE)], w_sem.at[2 * t]))
-        loads.append(pltpu.make_async_copy(wu.at[:, pl.ds(t * LANE, LANE)], wgu.at[t, :, pl.ds(LANE, LANE)], w_sem.at[2 * t + 1]))
-    loads.append(pltpu.make_async_copy(wd, wdn, w_sem.at[2 * tiles]))
+        loads.append(pltpu.make_async_copy(wg.at[:, pl.ds(t * LANE, LANE)], wgu.at[t, :, pl.ds(0, LANE)], w_sem.at[0]))
+        loads.append(pltpu.make_async_copy(wu.at[:, pl.ds(t * LANE, LANE)], wgu.at[t, :, pl.ds(LANE, LANE)], w_sem.at[0]))
+    loads.append(pltpu.make_async_copy(wd, wdn, w_sem.at[1]))
     table[...] = jnp.zeros_like(table)
     for copy in inputs[2:]:
         copy.wait()
@@ -96,35 +96,38 @@
     def piece_of(h):
         return pl.ds(h * span, span)
 
-    def lane_copy(i, p, src, dst, send, recv, device):
+    whole = pl.ds(0, width)
+
+    def lane_copy(i, cols, src, dst, send, recv, device):
         s = source(i)
-        return remote(xbuf.at[s, lane_rows(src), part_of(p)], xbuf.at[s, lane_rows(dst), part_of(p)],
-                      send.at[i, p], recv.at[i, p], device)
+        return remote(xbuf.at[s, lane_rows(src), cols], xbuf.at[s, lane_rows(dst), cols], send, recv, device)
 
     def across_copy(i, p):
-        return lane_copy(i, p, 0, 2, ys, yr, across)
-
-    def beside_copy(i, p):
-        return lane_copy(i, p, 0, 1, cs, cr, partner)
-
-    def forward_copy(i, p):
-        return lane_copy(i, p, 2, 3, fs, fr, partner)
+        return lane_copy(i, part_of(p), 0, 2, sent.at[0], yr.at[i, p], across)
+
+    def beside_copy(i, cols):
+        return lane_copy(i, cols, 0, 1, sent.at[1], cr.at[i], partner)
+
+    def forward_copy(i, cols):
+        return lane_copy(i, cols, 2, 3, sent.at[2], fr.at[i], partner)
 
     def source_copy(i, p, to, at):
         return remote(outgoing.at[i, :, part_of(p)], xbuf.at[at, lane_rows(0), part_of(p)],
-                      zs.at[i, p], zr.at[at, p], to * GROUP + j)
-
-    def give_copy(i, side, h):
-        return remote(give.at[i, side, :, piece_of(h)], take.at[i, side, :, piece_of(h)],
-                      gs.at[2 * i + side, h], gr.at[2 * i + side, h], partner)
+                      sent.at[3], zr.at[at, p], to * GROUP + j)
+
+    def low_give(i, cols):
+        return remote(give.at[i, 0, :, cols], take.at[i, 0, :, cols], sent.at[4], lr.at[i], partner)
+
+    def high_give(i, p):
+        return remote(give.at[i, 1, :, part_of(p)], take.at[i, 1, :, part_of(p)], sent.at[4], gr.at[i, p], partner)
 
     def cross_copy(i, h):
         return remote(cross.at[i, :, piece_of(h)], crossed.at[i, :, piece_of(h)],
-                      bs.at[i, h], br.at[i, h], across)
+                      sent.at[5], br.at[i, h], across)
 
     def return_copy(i, h, to, at):
         return remote(finished.at[i, :, piece_of(h)], ret.at[at, :, piece_of(h)],
-                      es.at[i, h], er.at[at, h], to * GROUP + j)
+                      sent.at[7 if i == n - 1 else 6], er.at[at, h], to * GROUP + j)
 
     def depart(i):
         for p in range(PARTS):
@@ -133,11 +136,11 @@
     def relay(i, p):
         source_copy(i, p, partner // GROUP, source(i)).wait_recv()
         across_copy(i, p).start()
-        beside_copy(i, p).start()
+        beside_copy(i, part_of(p)).start()
 
     def forward(i, p):
         across_copy(i, p).wait_recv()
-        forward_copy(i, p).start()
+        forward_copy(i, part_of(p)).start()
 
     def rise(i, side):
         rows = xbuf[source(i), lane_rows(2 * side, 2)]
@@ -148,16 +151,25 @@
             hidden[:, pl.ds(t * LANE, LANE)] = act.astype(jnp.bfloat16)
 
     def fall(i, side):
-        for h in pieces:
-            cols = piece_of(h)
-            piece = jnp.dot(hidden[...], wdn[:, cols], preferred_element_type=jnp.float32)
-            part[i, side, :, cols] = piece[0:cap]
-            give[i, side, :, cols] = piece[cap:2 * cap].astype(jnp.bfloat16)
-        for h in pieces:
-            give_copy(i, side, h).start()
+        for p in parts:
+            for h in groups[p]:
+                cols = piece_of(h)
+                piece = jnp.dot(hidden[...], wdn[:, cols], preferred_element_type=jnp.float32)
+                part[i, side, :, cols] = piece[0:cap]
+                give[i, side, :, cols] = piece[cap:2 * cap].astype(jnp.bfloat16)
+
+            @pl.when(side == 0)
+            def _():
+                low_give(i, part_of(p)).start()
+
+            @pl.when(side == 1)
+            def _():
+                high_give(i, p).start()
 
     def reduce_pair(i, h, send):
-        give_copy(i, 1, h).wait_recv()
+        for p in parts:
+            if h == groups[p][0]:
+                high_give(i, p).wait_recv()
         cols = piece_of(h)
         cross[i, :, cols] = (part[i, 1, :, cols] + take[i, 1, :, cols].astype(jnp.float32)).astype(jnp.bfloat16)
         if send:
@@ -168,7 +180,8 @@
             cross_copy(i, h).start()
 
     def finish(i, h):
-        give_copy(i, 0, h).wait_recv()
+        if h == 0:
+            low_give(i, whole).wait_recv()
         cross_copy(i, h).wait_recv()
         cols = piece_of(h)
         done = (part[i, 0, :, cols] + take[i, 0, :, cols].astype(jnp.float32)
@@ -200,7 +213,7 @@
                 term = total[:, cols] + term
             if last:
                 out[:, cols] = term.astype(jnp.bfloat16)
-                pltpu.make_async_copy(out.at[:, cols], out_to.at[:, cols], out_sem.at[h]).start()
+                pltpu.make_async_copy(out.at[:, cols], out_to.at[:, cols], out_sem.at[0]).start()
             else:
                 total[:, cols] = term
 
@@ -219,13 +232,14 @@
 
     pieces = range(PIECES)
     parts = range(PARTS)
+    groups = [pieces[p * PIECES // PARTS:(p + 1) * PIECES // PARTS] for p in parts]
     at_edge, within = edge == 0, edge > 0
     pack(g, xbuf.at[g, lane_rows(0)])
-    pack(source(1), outgoing.at[1])
     pl.semaphore_wait(barrier, len(others))
     for p in parts:
         across_copy(0, p).start()
-        beside_copy(0, p).start()
+        beside_copy(0, part_of(p)).start()
+    pack(source(1), outgoing.at[1])
     depart(1)
     for i in range(2, n):
         pack(source(i), outgoing.at[i])
@@ -233,8 +247,8 @@
         @pl.when(within)
         def _():
             depart(i)
-    for load in loads:
-        load.wait()
+    pltpu.make_async_copy(wgu, wgu, w_sem.at[0]).wait()
+    loads[-1].wait()
 
     def step(k, carry):
         def at(c):
@@ -281,10 +295,11 @@
                     for p in parts:
                         forward(o - 1, p)
 
-                @pl.when(within)
-                def _():
-                    for p in parts:
-                        relay(o, p)
+                if o > 3:
+                    @pl.when(within)
+                    def _():
+                        for p in parts:
+                            relay(o, p)
 
             @at(2 * o)
             def _():
@@ -313,13 +328,11 @@
 
         @pl.when(side == 0)
         def _():
-            for p in parts:
-                beside_copy(i, p).wait_recv()
+            beside_copy(i, whole).wait_recv()
 
         @pl.when(side == 1)
         def _():
-            for p in parts:
-                forward_copy(i, p).wait_recv()
+            forward_copy(i, whole).wait_recv()
         rise(i, side)
 
         @at(2 * n - 1)
@@ -330,12 +343,31 @@
         for o in range(n - 1):
             @at(6 if o == 0 else 3 if o == 1 else 5 if o == 2 else 2 * o + 2)
             def _():
-                for h in pieces:
+                for h in pieces[len(groups[0]):] if 0 < o < 3 else pieces:
                     reduce_pair(o, h, o > 0)
         fall(i, side)
+        for o in (1, 2):
+            @at(2 * o)
+            def _():
+                if o == 2:
+                    @pl.when(within)
+                    def _():
+                        for p in parts:
+                            relay(3, p)
+                for h in groups[0]:
+                    reduce_pair(o, h, True)
         return carry
 
     lax.fori_loop(0, 2 * n, step, 0)
+    def drain():
+        lane = [xbuf.at[:, lane_rows(k)] for k in range(3)]
+        left = pl.ds(1, n - 1)
+        for k, (src, dst) in enumerate([
+                (lane[0], lane[2]), (lane[0], lane[1]), (lane[2], lane[1]),
+                (outgoing.at[left], outgoing.at[left]), (give, take), (cross, crossed),
+                (finished.at[pl.ds(1, n - 2)], ret.at[pl.ds(1, n - 2)])]):
+            remote(src, dst, sent.at[k], yr.at[0, 0], partner).wait_send()
+
     @pl.when(at_edge)
     def _():
         for h in pieces:
@@ -343,6 +375,7 @@
         own(True, False)
         for h in pieces:
             finish(n - 1, h)
+        drain()
         mixers = [mixer(i) for i in range(1, n)]
         for h in pieces:
             for mix in mixers:
@@ -361,21 +394,9 @@
         for i in range(1, n):
             mix_all(i, i == 1, False)
         own(False, True)
-    for h in pieces:
-        pltpu.make_async_copy(out.at[:, piece_of(h)], out_to.at[:, piece_of(h)], out_sem.at[h]).wait()
-    for i in range(n):
-        for p in parts:
-            across_copy(i, p).wait_send()
-            beside_copy(i, p).wait_send()
-            forward_copy(i, p).wait_send()
-            if i:
-                source_copy(i, p, source(i), g).wait_send()
-        for h in pieces:
-            give_copy(i, 0, h).wait_send()
-            give_copy(i, 1, h).wait_send()
-            cross_copy(i, h).wait_send()
-            if i:
-                return_copy(i, h, source(i), g).wait_send()
+        drain()
+    remote(finished.at[n - 1], ret.at[0], sent.at[7], er.at[0, 0], partner).wait_send()
+    pltpu.make_async_copy(out, out_to, out_sem.at[0]).wait()
 
 
 def per_device(tokens, routing, gates, norm_gain, w_gate, w_up, w_down):
@@ -387,9 +408,7 @@
     cap = -(-cap // 16) * 16
     ff = w_gate.shape[2]
     bf, f32 = jnp.bfloat16, jnp.float32
-    by_part = pltpu.SemaphoreType.DMA((n, PARTS))
-    by_side = pltpu.SemaphoreType.DMA((2 * n, PIECES))
-    by_piece = pltpu.SemaphoreType.DMA((n, PIECES))
+    dma = pltpu.SemaphoreType.DMA
     hbm = pl.BlockSpec(memory_space=pl.ANY)
     return pl.pallas_call(
         functools.partial(kernel, n, cap),
@@ -419,10 +438,9 @@
             pltpu.VMEM((LANE, toks), f32),
             pltpu.VMEM((toks, LANE), f32),
             pltpu.VMEM((toks, LANE), f32),
-            pltpu.SemaphoreType.DMA((4,)),
-            pltpu.SemaphoreType.DMA((2 * (ff // LANE) + 1,)),
-            pltpu.SemaphoreType.DMA((PIECES,)),
-        ] + [by_part] * 8 + [by_side] * 2 + [by_piece] * 4,
+            dma((4,)), dma((2,)), dma((1,)), dma((8,)), dma((n, PARTS)), dma((n, PARTS)), dma((n,)), dma((n,)),
+            dma((n,)), dma((n, PARTS)), dma((n, PIECES)), dma((n, PIECES)),
+        ],
         compiler_params=pltpu.CompilerParams(
             collective_id=0, has_side_effects=True, vmem_limit_bytes=62 * 1024 * 1024),
     )(tokens, routing.T, gates.T, norm_gain, w_gate.reshape(w_gate.shape[1:]),

time: 73.6 us -> 71.4 us (0.970)
  Pallas kernels: 71.5 us -> 69.4 us
    pallas_call x1, Pallas kernels: 71.5 us -> 69.4 us  [per_device(): pl.pallas_call(functools.partial(kernel, n, cap), out_shape=jax.ShapeDtyp...]
where the time goes in v3:
time: 71.4 us; the launch traced here: 71.3 us
  Pallas kernels  69.4 us (97%)
  local copies, waits for them, and re-layouts  1.88 us (3%)
    pallas_call x1, Pallas kernels, per_device(): pl.pallas_call(functools.partial(kernel, n, cap), out_shape=jax.ShapeDtyp...  69.4 us
    unnamed x1, local copies, waits for them, and re-layouts  1.88 us

profile of v3, /device:TPU:0, one launch (start us, length us, event | category | flops | bytes accessed | tf_op | source)
XLA Modules:
  0.0 71.3 jit_solution(12991013888399811097)
XLA Ops:
  0.0 69.4 %shard_map.73 = bf16[128,2048]{1,0:T(8,128)(2,1)} custom-call(bf16[128,2048]{1,0:T(8,128)(2,1)} %tok_in.1, s32[2,128]{1,0:T(2,128)} %bitcast.8, f32[2,128]{1,0:T(2,128)} %bitcast.9, bf16[2048]{0:T(1024)(128)(2,1)} %gain_in.1, bf16[2048,896]{1,0:T(8,128)(2,1)} %bitcast.5, bf16[2048,896]{1,0:T(8,128)(2,1)} %bitcast.6, bf16[896,2048]{1,0:T(8,128)(2,1)} %bitcast.7), custom_call_target="tpu_custom_call" | custom-call | tf_op jit(solution)/shard_map/pallas_call | solution.py:413
  69.4 1.9 %copy.9 = bf16[128,2048]{1,0:T(8,128)(2,1)} copy(bf16[128,2048]{1,0:T(8,128)(2,1)} %shard_map.73) | data formatting | bytes 1048576

commit v4 on v3

--- a/solution.py
+++ b/solution.py
@@ -15,7 +15,7 @@
 
 def kernel(n, cap, tok_in, rt_in, gt_in, gain_in, wg, wu, wd, out_to,
            tok, rt, gt, gain, out, normed, outgoing, xbuf, wgu, wdn, hidden, part, give, take, cross, crossed,
-           finished, ret, total, table, turned, code, in_sem, w_sem, out_sem,
+           finished, ret, total, table, turned, code, sums, in_sem, w_sem, out_sem,
            sent, zr, yr, cr, fr, lr, gr, br, er):
     toks, width = tok.shape
     ff = wg.shape[1]
@@ -111,6 +111,9 @@
     def forward_copy(i, cols):
         return lane_copy(i, cols, 2, 3, sent.at[2], fr.at[i], partner)
 
+    def last_forward(p):
+        return lane_copy(n - 1, part_of(p), 2, 3, sent.at[2], fr.at[n - 1 + p], partner)
+
     def source_copy(i, p, to, at):
         return remote(outgoing.at[i, :, part_of(p)], xbuf.at[at, lane_rows(0), part_of(p)],
                       sent.at[3], zr.at[at, p], to * GROUP + j)
@@ -149,6 +152,25 @@
             gate_act, up_act = both[:, :LANE], both[:, LANE:]
             act = gate_act / (1.0 + jnp.exp(-gate_act)) * up_act
             hidden[:, pl.ds(t * LANE, LANE)] = act.astype(jnp.bfloat16)
+
+    def rise_last():
+        rows = xbuf.at[source(n - 1), lane_rows(2, 2)]
+        for p in range(PARTS):
+            across_copy(n - 1, p).wait_recv()
+            last_forward(p).start()
+            last_forward(p).wait_recv()
+            block = rows[:, part_of(p)]
+            for t in range(tiles):
+                both = jnp.dot(block, wgu[t, part_of(p)], preferred_element_type=jnp.float32)
+                cols = pl.ds(t * 2 * LANE, 2 * LANE)
+                if p:
+                    both = sums[:, cols] + both
+                if p < PARTS - 1:
+                    sums[:, cols] = both
+                else:
+                    gate_act, up_act = both[:, :LANE], both[:, LANE:]
+                    act = gate_act / (1.0 + jnp.exp(-gate_act)) * up_act
+                    hidden[:, pl.ds(t * LANE, LANE)] = act.astype(jnp.bfloat16)
 
     def fall(i, side):
         for p in parts:
@@ -175,8 +197,8 @@
         if send:
             cross_copy(i, h).start()
 
-    def send_cross(i):
-        for h in pieces:
+    def send_cross(i, some):
+        for h in some:
             cross_copy(i, h).start()
 
     def finish(i, h):
@@ -316,16 +338,6 @@
                     for p in parts[1:]:
                         relay(o, p)
 
-        @at(2 * n - 1)
-        def _():
-            @pl.when(at_edge)
-            def _():
-                send_cross(0)
-                for h in pieces:
-                    finish(n - 2, h)
-            for p in parts:
-                forward(n - 1, p)
-
         @pl.when(side == 0)
         def _():
             beside_copy(i, whole).wait_recv()
@@ -335,11 +347,6 @@
             forward_copy(i, whole).wait_recv()
         rise(i, side)
 
-        @at(2 * n - 1)
-        def _():
-            @pl.when(within)
-            def _():
-                finish(n - 2, 0)
         for o in range(n - 1):
             @at(6 if o == 0 else 3 if o == 1 else 5 if o == 2 else 2 * o + 2)
             def _():
@@ -358,7 +365,26 @@
                     reduce_pair(o, h, True)
         return carry
 
-    lax.fori_loop(0, 2 * n, step, 0)
+    lax.fori_loop(0, 2 * n - 1, step, 0)
+
+    first, last = pieces[:-2], PIECES - 1
+    odd = j % 2 == 1
+
+    @pl.when(at_edge)
+    def _():
+        send_cross(0, first)
+
+        @pl.when(odd)
+        def _():
+            send_cross(0, [last - 1])
+        for h in pieces:
+            finish(n - 2, h)
+    rise_last()
+
+    @pl.when(within)
+    def _():
+        finish(n - 2, 0)
+    fall(n - 1, 1)
     def drain():
         lane = [xbuf.at[:, lane_rows(k)] for k in range(3)]
         left = pl.ds(1, n - 1)
@@ -372,13 +398,23 @@
     def _():
         for h in pieces:
             reduce_pair(n - 1, h, True)
-        own(True, False)
+        @pl.when(jnp.logical_not(odd))
+        def _():
+            send_cross(0, [last - 1])
+        send_cross(0, [last])
+        mixers = [mixer(i) for i in range(n)]
+        for h in first:
+            finish(0, h)
+            mixers[0](h, True, False)
         for h in pieces:
             finish(n - 1, h)
-        drain()
-        mixers = [mixer(i) for i in range(1, n)]
-        for h in pieces:
-            for mix in mixers:
+        for h in pieces:
+            if h not in first:
+                finish(0, h)
+                mixers[0](h, True, False)
+            if h == last:
+                drain()
+            for mix in mixers[1:]:
                 mix(h, False, mix is mixers[-1])
 
     @pl.when(within)
@@ -386,7 +422,7 @@
         finish(n - 2, 1)
         for h in pieces:
             reduce_pair(n - 1, h, True)
-        send_cross(0)
+        send_cross(0, pieces)
         for h in pieces[2:]:
             finish(n - 2, h)
         for h in pieces:
@@ -438,7 +474,8 @@
             pltpu.VMEM((LANE, toks), f32),
             pltpu.VMEM((toks, LANE), f32),
             pltpu.VMEM((toks, LANE), f32),
-            dma((4,)), dma((2,)), dma((1,)), dma((8,)), dma((n, PARTS)), dma((n, PARTS)), dma((n,)), dma((n,)),
+            pltpu.VMEM((2 * cap, 2 * ff), f32),
+            dma((4,)), dma((2,)), dma((1,)), dma((8,)), dma((n, PARTS)), dma((n, PARTS)), dma((n,)), dma((n - 1 + PARTS,)),
             dma((n,)), dma((n, PARTS)), dma((n, PIECES)), dma((n, PIECES)),
         ],
         compiler_params=pltpu.CompilerParams(

time: 71.4 us -> 71.4 us (level)
  no operation moved by 1% of the time
where the time goes in v4:
time: 71.4 us; the launch traced here: 71.2 us
  Pallas kernels  69.4 us (97%)
  local copies, waits for them, and re-layouts  1.88 us (3%)
    pallas_call x1, Pallas kernels, per_device(): pl.pallas_call(functools.partial(kernel, n, cap), out_shape=jax.ShapeDtyp...  69.4 us
    unnamed x1, local copies, waits for them, and re-layouts  1.88 us

profile of v4, /device:TPU:0, one launch (start us, length us, event | category | flops | bytes accessed | tf_op | source)
XLA Modules:
  0.0 71.2 jit_solution(13127686055766633395)
XLA Ops:
  0.0 69.4 %shard_map.73 = bf16[128,2048]{1,0:T(8,128)(2,1)} custom-call(bf16[128,2048]{1,0:T(8,128)(2,1)} %tok_in.1, s32[2,128]{1,0:T(2,128)} %bitcast.8, f32[2,128]{1,0:T(2,128)} %bitcast.9, bf16[2048]{0:T(1024)(128)(2,1)} %gain_in.1, bf16[2048,896]{1,0:T(8,128)(2,1)} %bitcast.5, bf16[2048,896]{1,0:T(8,128)(2,1)} %bitcast.6, bf16[896,2048]{1,0:T(8,128)(2,1)} %bitcast.7), custom_call_target="tpu_custom_call" | custom-call | tf_op jit(solution)/shard_map/pallas_call | solution.py:449
  69.4 1.9 %copy.9 = bf16[128,2048]{1,0:T(8,128)(2,1)} copy(bf16[128,2048]{1,0:T(8,128)(2,1)} %shard_map.73) | data formatting | bytes 1048576
